TPU v7x, 32 devices: a whole 2x2x4 slice. The times are simulated.
32 devices in a mesh: grp: 2 (over y), sp: 4 (over z), tp: 4 (over x, core).
Axes of the slice: x: 2, y: 2, z: 4, core: 2. Of those that a mesh axis runs over, the one named last changes fastest.
Arguments:
- tokens: bfloat16 [3072, 2048], P(('grp', 'sp')), parts along dimension 0, may hold values from -6 to 6
- norm_gain: float32 [2, 2048], replicated, may hold values from 0.1 to 1.9
- entry_weight: bfloat16 [2, 2048, 2048], P(None, 'sp', 'tp'), may hold values from -0.125 to 0.125
- mix_weight: bfloat16 [2, 4, 512, 512], P(None, 'tp'), may hold values from -0.25 to 0.25
- pool_gain: float32 [2, 2048], P(None, 'tp'), may hold values from 0.1 to 1.9
- back_weight: bfloat16 [2, 2048, 2048], P(None, 'tp', 'sp'), may hold values from -0.25 to 0.25
Outputs:
- result_tokens: bfloat16 [3072, 2048], P(('grp', 'sp')), parts along dimension 0
There are 2 independent parts, one for each index of `grp`. A program takes and returns all parts, laid end to end along the dimension named above; an argument that names none is the same for every part. Nothing has to cross between parts.
All inputs are finite; a program needn't handle non-finite values.
Results may differ from a plain program's by a relative error of at most 0.018.
Values may be sent and summed in bfloat16 or wider, within the bound.
A program may use at most 64 MiB of HBM per device.

v0:
```python
import jax
import jax.numpy as jnp
from jax import lax
from jax.sharding import PartitionSpec as P

GROUPS = 4
LAYERS = 2
EPSILON = 1e-05


def extended_2(value, sides, width):
    for axis, dim in sides:
        size, length = (lax.axis_size(axis), value.shape[dim])
        up = [(i, (i + 1) % size) for i in range(size - 1)]
        down = [(j, i) for i, j in up]
        last = lax.slice_in_dim(value, length - width, length, axis=dim)
        first = lax.slice_in_dim(value, 0, width, axis=dim)
        before = lax.ppermute(last, axis, up)
        after = lax.ppermute(first, axis, down)
        value = jnp.concatenate([before, value, after], axis=dim)
    return value


def window_mean(padded, positions, halves, total_length, reach):
    row_count = positions.shape[0]
    summed = jnp.zeros((row_count,) + padded.shape[1:], jnp.float32)
    for offset in range(-reach, reach):
        inside = ((offset >= -halves) & (offset < halves)).astype(jnp.float32)
        summed = (
            summed + padded[reach + offset : reach + offset + row_count] * inside[None, :, None]
        )
    lower = jnp.maximum(positions[:, None] - halves[None, :], 0)
    upper = jnp.minimum(positions[:, None] + halves[None, :], total_length)
    counted = (upper - lower).astype(jnp.float32)
    return summed / counted[:, :, None]


def normalize(state, gain):
    values = state.astype(jnp.float32)
    scaled = values * lax.rsqrt(jnp.mean(values * values, axis=-1, keepdims=True) + EPSILON)
    return (scaled * gain).astype(jnp.bfloat16)


def pool_groups(pooled_in, mix_layer, gain_layer, reach):
    row_count = pooled_in.shape[0]
    group_here = mix_layer.shape[0]
    width = mix_layer.shape[1]
    extended = extended_2(pooled_in, (("sp", 0),), reach)
    first_group = lax.axis_index("tp") * group_here
    halves = jnp.left_shift(jnp.int32(1), first_group + jnp.arange(group_here, dtype=jnp.int32))
    positions = lax.axis_index("sp") * row_count + jnp.arange(row_count, dtype=jnp.int32)
    total_length = lax.axis_size("sp") * row_count
    padded = extended.reshape(row_count + 2 * reach, group_here, width).astype(jnp.float32)
    means = window_mean(padded, positions, halves, total_length, reach)
    differ = (means - padded[reach : reach + row_count]).astype(jnp.bfloat16)
    mixed = jnp.einsum("tgc,gcd->tgd", differ, mix_layer, preferred_element_type=jnp.float32)
    return (mixed.reshape(row_count, group_here * width) * gain_layer).astype(jnp.bfloat16)


def per_device(tokens, norm_gain, entry_weight, mix_weight, pool_gain, back_weight):
    reach = 2 ** (GROUPS - 1)
    state = tokens
    entry_all, back_all = (
        lax.all_gather(entry_weight, "sp", axis=1, tiled=True),
        lax.all_gather(back_weight, "sp", axis=2, tiled=True),
    )
    for layer in range(LAYERS):
        normed = normalize(state, norm_gain[layer])
        pooled_in = jnp.dot(normed, entry_all[layer], preferred_element_type=jnp.float32).astype(
            jnp.bfloat16
        )
        back_local = back_all[layer]
        mixed = pool_groups(pooled_in, mix_weight[layer], pool_gain[layer], reach)
        update = jnp.dot(mixed, back_local, preferred_element_type=jnp.float32)
        summed = lax.psum(update.astype(jnp.bfloat16), "tp").astype(jnp.float32)
        state = (state.astype(jnp.float32) + summed).astype(jnp.bfloat16)
    return state


def solution(mesh):
    return jax.shard_map(
        per_device,
        mesh=mesh,
        in_specs=(
            P(("grp", "sp"), None),
            P(),
            P(None, "sp", "tp"),
            P(None, "tp", None, None),
            P(None, "tp"),
            P(None, "tp", "sp"),
        ),
        out_specs=P(("grp", "sp"), None),
        check_vma=False,
    )
```

profile of v0, /device:TPU:0, one launch (start us, length us, event | category | flops | bytes accessed | tf_op | source)
XLA Modules:
  0.0 298.0 jit_solution(13952838582287595426)
XLA Ops:
  6.5 0.0 copy-start
  6.5 0.0 copy-start.3
  6.5 0.0 copy-start.2
  6.5 0.0 all-gather.3.cloned.1.call-start
  6.5 0.7 all-gather.3.cloned.1.call-update
  7.3 0.0 all-gather.5.cloned.1.call-start
  7.3 0.7 all-gather.5.cloned.1.call-update
  8.0 0.0 all-reduce.3.cloned.1.call-start
  8.1 0.0 copy-done
  8.1 0.4 fusion
  8.5 0.0 copy-done.3
  8.5 0.0 copy-done.2
  8.5 83.9 %all-gather.3.cloned.1.call-done = bf16[2,2048,512]{2,1,0:T(8,128)(2,1)} async-done(((bf16[2,512,512]{2,1,0:T(8,128)(2,1)}), bf16[2,2048,512]{2,1,0:T(8,128)(2,1)}) %all-gather.3.cloned.1.call-update) | async-done | bytes 4194320 | tf_op jit(solution)/shard_map/all_gather | solution.py:64
  92.4 2.6 fusion.20
  95.0 1.3 collective-permute-start
  96.3 1.3 collective-permute-start.1
  97.8 0.0 collective-permute-done
  97.8 4.2 %collective-permute-done.1 = bf16[8,512]{1,0:T(8,128)(2,1)S(1)} collective-permute-done((bf16[8,512]{1,0:T(8,128)(2,1)S(1)}, bf16[8,512]{1,0:T(8,128)(2,1)S(1)}, u32[]{:S(2)}, u32[]{:S(2)}) %collective-permute-start.1) | collective-permute-done | bytes 8224 | tf_op jit(solution)/shard_map/ppermute | solution.py:19
  101.9 0.1 maximum_convert_fusion
  102.0 71.2 %all-gather.5.cloned.1.call-done = bf16[2,512,2048]{2,1,0:T(8,128)(2,1)} async-done(((bf16[2,512,512]{2,1,0:T(8,128)(2,1)}), bf16[2,512,2048]{2,1,0:T(8,128)(2,1)}) %all-gather.5.cloned.1.call-update) | async-done | bytes 4194320 | tf_op jit(solution)/shard_map/all_gather | solution.py:65
  173.2 5.3 %convolution_convert_fusion.1 = bf16[384,2048]{1,0:T(8,128)(2,1)} fusion(bf16[2,512,2048]{2,1,0:T(8,128)(2,1)} %all-gather.5.cloned.1.call-done, bf16[2,1,512,512]{3,2,1,0:T(8,128)(2,1)} %param.9, f32[512]{0:T(512)S(1)} %bitcast.87, f32[400,1,512]{2,0,1:T(8,128)S(1)} %maximum_convert_fusion, f32[384]{0:T(512)S(1)} %subtract_convert_fusion, f32[]{:T(128)S(6)} %mul.373, ...), kind=kOutput, calls=%fused_computation.15 | convolution fusion | flops 1014497280 | bytes 16781376 | tf_op jit(solution)/shard_map/dot_general | solution.py:74
  178.5 0.0 all-reduce.3.cloned.1.call-update
  178.5 0.0 all-reduce.5.cloned.1.call-start
  178.6 41.4 %all-reduce.3.cloned.1.call-done = bf16[384,2048]{1,0:T(8,128)(2,1)} async-done(((bf16[384,2048]{1,0:T(8,128)(2,1)}), bf16[384,2048]{1,0:T(8,128)(2,1)}) %all-reduce.3.cloned.1.call-update) | async-done | bytes 1572880 | tf_op jit(solution)/shard_map/psum | solution.py:75
  220.0 0.0 copy-start.1
  220.0 2.1 fusion.4
  222.1 0.0 copy-done.1
  222.1 2.6 fusion.23
  224.8 3.4 %collective-permute-start.2 = (bf16[8,512]{1,0:T(8,128)(2,1)S(1)}, bf16[8,512]{1,0:T(8,128)(2,1)S(1)}, u32[]{:S(2)}, u32[]{:S(2)}) collective-permute-start(bf16[8,512]{1,0:T(8,128)(2,1)S(1)} %get-tuple-element.5), channel_id=1, source_target_pairs={{0,4},{4,8},{8,12},{1,5},{5,9},{9,13},{2,6},{6,10},{10,14},{3,7},{... | collective-permute-start | bytes 24584 | tf_op jit(solution)/shard_map/ppermute | solution.py:18
  228.2 1.3 collective-permute-start.3
  229.5 0.0 collective-permute-done.2
  229.5 4.2 %collective-permute-done.3 = bf16[8,512]{1,0:T(8,128)(2,1)S(1)} collective-permute-done((bf16[8,512]{1,0:T(8,128)(2,1)S(1)}, bf16[8,512]{1,0:T(8,128)(2,1)S(1)}, u32[]{:S(2)}, u32[]{:S(2)}) %collective-permute-start.3) | collective-permute-done | bytes 8224 | tf_op jit(solution)/shard_map/ppermute | solution.py:19
  233.7 1.0 maximum_convert_fusion.1
  234.7 11.3 %convolution_convert_fusion = bf16[384,2048]{1,0:T(8,128)(2,1)} fusion(bf16[2,512,2048]{2,1,0:T(8,128)(2,1)} %all-gather.5.cloned.1.call-done, bf16[2,1,512,512]{3,2,1,0:T(8,128)(2,1)} %param.9, f32[512]{0:T(512)S(1)} %bitcast.86, f32[400,1,512]{2,0,1:T(8,128)} %maximum_convert_fusion.1, f32[384]{0:T(512)S(1)} %subtract_convert_fusion, f32[]{:T(128)S(6)} %mul.373, ...), kind=kOutput, calls=%fused_computation.14 | convolution fusion | flops 1014497280 | bytes 16780864 | tf_op jit(solution)/shard_map/dot_general | solution.py:74
  246.0 0.0 all-reduce.5.cloned.1.call-update
  246.0 42.1 %all-reduce.5.cloned.1.call-done = bf16[384,2048]{1,0:T(8,128)(2,1)} async-done(((bf16[384,2048]{1,0:T(8,128)(2,1)}), bf16[384,2048]{1,0:T(8,128)(2,1)}) %all-reduce.5.cloned.1.call-update) | async-done | bytes 1572880 | tf_op jit(solution)/shard_map/psum | solution.py:75
  288.2 3.4 %fusion.7 = bf16[384,2048]{1,0:T(8,128)(2,1)} fusion(bf16[384,2048]{1,0:T(8,128)(2,1)} %all-reduce.5.cloned.1.call-done, bf16[384,2048]{1,0:T(8,128)(2,1)S(1)} %copy-done.1, bf16[384,2048]{1,0:T(8,128)(2,1)S(1)} %copy-done), kind=kLoop, calls=%fused_computation.13 | loop fusion | flops 6291456 | bytes 6291456 | tf_op jit(solution)/shard_map/convert_element_type | solution.py:76
  (7 shorter events, 0.1 us)
Async XLA Ops:
  6.5 1.5 copy-start
  6.5 1.9 copy-start.3
  6.5 2.0 copy-start.2
  6.5 85.9 %all-gather.3.cloned.1.call-start = ((), (), s32[]{:S(2)}) async-start(), calls=%async_computation | async-start | bytes 5242880 | tf_op jit(solution)/shard_map/all_gather | solution.py:64
  7.3 166.0 %all-gather.5.cloned.1.call-start = ((), (), s32[]{:S(2)}) async-start(), calls=%async_computation.1 | async-start | bytes 5242880 | tf_op jit(solution)/shard_map/all_gather | solution.py:65
  8.0 212.0 %all-reduce.3.cloned.1.call-start = ((), (), s32[]{:S(2)}) async-start(), calls=%async_computation.2 | async-start | bytes 3145728 | tf_op jit(solution)/shard_map/psum | solution.py:75
  95.0 2.7 collective-permute-start
  96.3 5.6 %collective-permute-start.1 = (bf16[8,512]{1,0:T(8,128)(2,1)S(1)}, bf16[8,512]{1,0:T(8,128)(2,1)S(1)}, u32[]{:S(2)}, u32[]{:S(2)}) collective-permute-start(bf16[8,512]{1,0:T(8,128)(2,1)S(1)} %get-tuple-element.8), channel_id=1, source_target_pairs={{4,0},{8,4},{12,8},{5,1},{9,5},{13,9},{6,2},{10,6},{14,10},{7,3},{... | collective-permute-start | bytes 24584 | tf_op jit(solution)/shard_map/ppermute | solution.py:19
  178.5 109.6 %all-reduce.5.cloned.1.call-start = ((), (), s32[]{:S(2)}) async-start(), calls=%async_computation.3 | async-start | bytes 3145728 | tf_op jit(solution)/shard_map/psum | solution.py:75
  220.0 2.1 copy-start.1
  224.8 4.7 %collective-permute-start.2 = (bf16[8,512]{1,0:T(8,128)(2,1)S(1)}, bf16[8,512]{1,0:T(8,128)(2,1)S(1)}, u32[]{:S(2)}, u32[]{:S(2)}) collective-permute-start(bf16[8,512]{1,0:T(8,128)(2,1)S(1)} %get-tuple-element.5), channel_id=1, source_target_pairs={{0,4},{4,8},{8,12},{1,5},{5,9},{9,13},{2,6},{6,10},{10,14},{3,7},{... | collective-permute-start | bytes 24584 | tf_op jit(solution)/shard_map/ppermute | solution.py:18
  228.2 5.5 %collective-permute-start.3 = (bf16[8,512]{1,0:T(8,128)(2,1)S(1)}, bf16[8,512]{1,0:T(8,128)(2,1)S(1)}, u32[]{:S(2)}, u32[]{:S(2)}) collective-permute-start(bf16[8,512]{1,0:T(8,128)(2,1)S(1)} %get-tuple-element.6), channel_id=1, source_target_pairs={{4,0},{8,4},{12,8},{5,1},{9,5},{13,9},{6,2},{10,6},{14,10},{7,3},{... | collective-permute-start | bytes 24584 | tf_op jit(solution)/shard_map/ppermute | solution.py:19
Sparse Core Ops, SparseCore 0:
  8.9 83.4 all-gather.2
  94.0 79.2 all-gather.4
  178.6 41.3 all-reduce.2
  246.1 41.9 all-reduce.4
where the time goes:
time: 298 us
  waiting for transfers between devices  249 us (84%)
  matrix products  21.8 us (7%)
  between operations  13.4 us (4%)
  starting transfers between devices  7.37 us (2%)
  other arithmetic  6.97 us (2%)
    all_gather x1, waiting for transfers between devices, per_device(): lax.all_gather(entry_weight, 'sp', axis=1, tiled=True)  83.9 us
    psum x2, waiting for transfers between devices, per_device(): summed = lax.psum(update.astype(jnp.bfloat16), 'tp').astype(jnp.float32)  83.6 us
    all_gather x1, waiting for transfers between devices, per_device(): lax.all_gather(back_weight, 'sp', axis=2, tiled=True)  71.2 us
    dot_general x2, matrix products, per_device(): update = jnp.dot(mixed, back_local, preferred_element_type=jnp.float32)  16.5 us
    ppermute x2, waiting for transfers between devices, extended_2(): after = lax.ppermute(first, axis, down)  8.37 us
  transfers between devices with their start and end apart: 8, of which 6 were waited for; matrix products, arithmetic and copies ran while one was open for 1% of the time, Pallas kernels for 0%

commit v1 on v0

--- a/solution.py
+++ b/solution.py
@@ -62,7 +62,7 @@
     state = tokens
     entry_all, back_all = (
         lax.all_gather(entry_weight, "sp", axis=1, tiled=True),
-        lax.all_gather(back_weight, "sp", axis=2, tiled=True),
+        jnp.concatenate(lax.all_gather(back_weight, "sp"), axis=2),
     )
     for layer in range(LAYERS):
         normed = normalize(state, norm_gain[layer])

time: 298 us -> 309 us (1.037)
  local copies, waits for them, and re-layouts: 0.04 us -> 14 us
  waiting for transfers between devices: 249 us -> 241 us
  starting transfers between devices: 7.37 us -> 11.8 us
    slice x0 -> x3, local copies, waits for them, and re-layouts: none -> 12.8 us  [per_device(): back_local = back_all[layer]]
    ppermute x2, waiting for transfers between devices: 8.37 us -> 0.01 us  [extended_2(): after = lax.ppermute(first, axis, down)]
    ppermute x2, starting transfers between devices: 4.67 us -> 9.09 us  [extended_2(): before = lax.ppermute(last, axis, up)]
  transfers between devices with their start and end apart: 8 -> 8, of which waited for: 6 -> 4; matrix products, arithmetic and copies ran while one was open for 1% -> 5% of each run, Pallas kernels for 0% -> 0%
where the time goes in v1:
time: 309 us
  waiting for transfers between devices  241 us (78%)
  matrix products  22.3 us (7%)
  local copies, waits for them, and re-layouts  14 us (5%)
  between operations  13.4 us (4%)
  starting transfers between devices  11.8 us (4%)
  other arithmetic  7.01 us (2%)
    psum x2, waiting for transfers between devices, per_device(): summed = lax.psum(update.astype(jnp.bfloat16), 'tp').astype(jnp.float32)  83.6 us
    all_gather x1, waiting for transfers between devices, per_device(): lax.all_gather(entry_weight, 'sp', axis=1, tiled=True)  83.2 us
    all_gather x1, waiting for transfers between devices, per_device(): lax.all_gather(back_weight, 'sp')  72.3 us
    dot_general x2, matrix products, per_device(): update = jnp.dot(mixed, back_local, preferred_element_type=jnp.float32)  17.1 us
    slice x3, local copies, waits for them, and re-layouts, per_device(): back_local = back_all[layer]  12.8 us
    ppermute x2, starting transfers between devices, extended_2(): before = lax.ppermute(last, axis, up)  9.09 us
  transfers between devices with their start and end apart: 8, of which 4 were waited for; matrix products, arithmetic and copies ran while one was open for 5% of the time, Pallas kernels for 0%

profile of v1, /device:TPU:0, one launch (start us, length us, event | category | flops | bytes accessed | tf_op | source)
XLA Modules:
  0.0 309.0 jit_solution(2619314944814629742)
XLA Ops:
  6.5 0.0 copy-start
  6.5 0.0 copy-start.3
  6.5 0.0 copy-start.2
  6.5 0.0 all-gather.4.cloned.1.call-start
  6.5 0.7 all-gather.4.cloned.1.call-update
  7.3 0.0 all-gather.6.cloned.1.call-start
  7.3 0.7 all-gather.6.cloned.1.call-update
  8.0 0.0 all-reduce.3.cloned.1.call-start
  8.2 0.0 copy-done
  8.2 0.0 copy-start.4
  8.2 0.4 fusion
  8.6 0.0 copy-done.3
  8.6 0.5 fusion.87
  9.2 0.0 copy-done.2
  9.2 83.2 %all-gather.4.cloned.1.call-done = bf16[2,2048,512]{2,1,0:T(8,128)(2,1)} async-done(((bf16[2,512,512]{2,1,0:T(8,128)(2,1)}), bf16[2,2048,512]{2,1,0:T(8,128)(2,1)}) %all-gather.4.cloned.1.call-update) | async-done | bytes 4194320 | tf_op jit(solution)/shard_map/all_gather | solution.py:64
  92.4 2.6 fusion.20
  95.0 1.3 collective-permute-start.1
  96.3 4.5 %collective-permute-start = (bf16[8,512]{1,0:T(8,128)(2,1)S(1)}, bf16[8,512]{1,0:T(8,128)(2,1)S(1)}, u32[]{:S(2)}, u32[]{:S(2)}) collective-permute-start(bf16[8,512]{1,0:T(8,128)(2,1)S(1)} %get-tuple-element.9), channel_id=1, source_target_pairs={{0,4},{4,8},{8,12},{1,5},{5,9},{9,13},{2,6},{6,10},{10,14},{3,7},{... | collective-permute-start | bytes 24584 | tf_op jit(solution)/shard_map/ppermute | solution.py:18
  100.9 72.3 %all-gather.6.cloned.1.call-done = bf16[8,512,512]{2,1,0:T(8,128)(2,1)} async-done(((bf16[2,512,512]{2,1,0:T(8,128)(2,1)}), bf16[8,512,512]{2,1,0:T(8,128)(2,1)}) %all-gather.6.cloned.1.call-update) | async-done | bytes 4194320 | tf_op jit(solution)/shard_map/all_gather | solution.py:65
  173.2 4.5 %fusion.83 = (bf16[1,512,4,512]{3,1,0,2:T(8,128)(2,1)}, bf16[1,512,4,512]{3,1,0,2:T(8,128)(2,1)}) fusion(bf16[2,512,4,512]{3,1,0,2:T(8,128)(2,1)} %bitcast.79), kind=kLoop, calls=%fused_computation.113 | loop fusion | bytes 8388608 | tf_op jit(solution)/shard_map/slice | solution.py:72
  177.7 4.2 %copy.9 = bf16[1,512,4,512]{1,3,2,0:T(8,128)(2,1)} copy(bf16[1,512,4,512]{3,1,0,2:T(8,128)(2,1)} %get-tuple-element.5) | data formatting | bytes 4194304 | tf_op jit(solution)/shard_map/slice | solution.py:72
  181.9 0.0 collective-permute-done.1
  181.9 0.0 collective-permute-done
  181.9 0.1 maximum_convert_fusion
  182.0 0.0 copy-done.4
  182.0 5.3 %convolution_convert_fusion.1 = bf16[384,2048]{1,0:T(8,128)(2,1)} fusion(bf16[512,2048]{0,1:T(8,128)(2,1)} %bitcast.81, bf16[2,1,512,512]{3,2,1,0:T(8,128)(2,1)} %param.9, f32[512]{0:T(512)S(1)} %bitcast.91, f32[400,1,512]{2,0,1:T(8,128)S(1)} %maximum_convert_fusion, f32[384]{0:T(512)S(1)} %subtract_convert_fusion, f32[]{:T(128)S(6)} %mul.373, ...), kind=kOutput, calls=%fused_computation.15 | convolution fusion | flops 1014497280 | bytes 16781376 | tf_op jit(solution)/shard_map/dot_general | solution.py:74
  187.3 0.0 all-reduce.3.cloned.1.call-update
  187.3 0.0 all-reduce.5.cloned.1.call-start
  187.3 41.5 %all-reduce.3.cloned.1.call-done = bf16[384,2048]{1,0:T(8,128)(2,1)} async-done(((bf16[384,2048]{1,0:T(8,128)(2,1)}), bf16[384,2048]{1,0:T(8,128)(2,1)}) %all-reduce.3.cloned.1.call-update) | async-done | bytes 1572880 | tf_op jit(solution)/shard_map/psum | solution.py:75
  228.8 0.0 copy-start.1
  228.8 2.1 fusion.4
  230.9 0.0 copy-done.1
  230.9 2.6 fusion.23
  233.6 0.6 fusion.84
  234.2 1.3 collective-permute-start.3
  235.4 4.5 %collective-permute-start.2 = (bf16[8,512]{1,0:T(8,128)(2,1)}, bf16[8,512]{1,0:T(8,128)(2,1)S(1)}, u32[]{:S(2)}, u32[]{:S(2)}) collective-permute-start(bf16[8,512]{1,0:T(8,128)(2,1)} %get-tuple-element.7), channel_id=1, source_target_pairs={{0,4},{4,8},{8,12},{1,5},{5,9},{9,13},{2,6},{6,10},{10,14},{3,7},{... | collective-permute-start | bytes 24584 | tf_op jit(solution)/shard_map/ppermute | solution.py:18
  240.0 4.1 %copy.10 = bf16[1,512,4,512]{1,3,2,0:T(8,128)(2,1)} copy(bf16[1,512,4,512]{3,1,0,2:T(8,128)(2,1)} %get-tuple-element.6) | data formatting | bytes 4194304 | tf_op jit(solution)/shard_map/slice | solution.py:72
  244.1 0.0 collective-permute-done.3
  244.1 0.0 collective-permute-done.2
  244.1 1.0 maximum_convert_fusion.1
  245.2 11.8 %convolution_convert_fusion = bf16[384,2048]{1,0:T(8,128)(2,1)} fusion(bf16[512,2048]{0,1:T(8,128)(2,1)} %bitcast.80, bf16[2,1,512,512]{3,2,1,0:T(8,128)(2,1)} %param.9, f32[512]{0:T(512)} %bitcast.90, f32[400,1,512]{2,0,1:T(8,128)} %maximum_convert_fusion.1, f32[384]{0:T(512)} %copy-done.4, f32[]{:T(128)S(6)} %mul.373, f32[]{:T(128)S(6)} %mul.370, ...), kind=kOutput, calls=%fused_computation.14 | convolution fusion | flops 1014497280 | bytes 16781376 | tf_op jit(solution)/shard_map/dot_general | solution.py:74
  257.0 0.0 all-reduce.5.cloned.1.call-update
  257.0 42.1 %all-reduce.5.cloned.1.call-done = bf16[384,2048]{1,0:T(8,128)(2,1)} async-done(((bf16[384,2048]{1,0:T(8,128)(2,1)}), bf16[384,2048]{1,0:T(8,128)(2,1)}) %all-reduce.5.cloned.1.call-update) | async-done | bytes 1572880 | tf_op jit(solution)/shard_map/psum | solution.py:75
  299.1 3.4 %fusion.7 = bf16[384,2048]{1,0:T(8,128)(2,1)} fusion(bf16[384,2048]{1,0:T(8,128)(2,1)} %all-reduce.5.cloned.1.call-done, bf16[384,2048]{1,0:T(8,128)(2,1)S(1)} %copy-done.1, bf16[384,2048]{1,0:T(8,128)(2,1)S(1)} %copy-done), kind=kLoop, calls=%fused_computation.13 | loop fusion | flops 6291456 | bytes 6291456 | tf_op jit(solution)/shard_map/convert_element_type | solution.py:76
  (5 shorter events, 0.0 us)
Async XLA Ops:
  6.5 1.7 copy-start
  6.5 2.1 copy-start.3
  6.5 2.6 copy-start.2
  6.5 85.9 %all-gather.4.cloned.1.call-start = ((), (), s32[]{:S(2)}) async-start(), calls=%async_computation | async-start | bytes 5242880 | tf_op jit(solution)/shard_map/all_gather | solution.py:64
  7.3 166.0 %all-gather.6.cloned.1.call-start = ((), (), s32[]{:S(2)}) async-start(), calls=%async_computation.3 | async-start | bytes 5242880 | tf_op jit(solution)/shard_map/all_gather | solution.py:65
  8.0 220.8 %all-reduce.3.cloned.1.call-start = ((), (), s32[]{:S(2)}) async-start(), calls=%async_computation.1 | async-start | bytes 3145728 | tf_op jit(solution)/shard_map/psum | solution.py:75
  8.2 173.8 %copy-start.4 = (f32[384]{0:T(512)}, f32[384]{0:T(512)S(1)}, u32[]{:S(2)}) copy-start(f32[384]{0:T(512)S(1)} %subtract_convert_fusion) | copy-start | bytes 4612
  95.0 86.8 %collective-permute-start.1 = (bf16[8,512]{1,0:T(8,128)(2,1)S(1)}, bf16[8,512]{1,0:T(8,128)(2,1)S(1)}, u32[]{:S(2)}, u32[]{:S(2)}) collective-permute-start(bf16[8,512]{1,0:T(8,128)(2,1)S(1)} %get-tuple-element.10), channel_id=1, source_target_pairs={{4,0},{8,4},{12,8},{5,1},{9,5},{13,9},{6,2},{10,6},{14,10},{7,3},{... | collective-permute-start | bytes 24584 | tf_op jit(solution)/shard_map/ppermute | solution.py:19
  96.3 85.5 %collective-permute-start = (bf16[8,512]{1,0:T(8,128)(2,1)S(1)}, bf16[8,512]{1,0:T(8,128)(2,1)S(1)}, u32[]{:S(2)}, u32[]{:S(2)}) collective-permute-start(bf16[8,512]{1,0:T(8,128)(2,1)S(1)} %get-tuple-element.9), channel_id=1, source_target_pairs={{0,4},{4,8},{8,12},{1,5},{5,9},{9,13},{2,6},{6,10},{10,14},{3,7},{... | collective-permute-start | bytes 24584 | tf_op jit(solution)/shard_map/ppermute | solution.py:18
  187.3 111.8 %all-reduce.5.cloned.1.call-start = ((), (), s32[]{:S(2)}) async-start(), calls=%async_computation.2 | async-start | bytes 3145728 | tf_op jit(solution)/shard_map/psum | solution.py:75
  228.8 2.1 copy-start.1
  234.2 10.0 %collective-permute-start.3 = (bf16[8,512]{1,0:T(8,128)(2,1)}, bf16[8,512]{1,0:T(8,128)(2,1)S(1)}, u32[]{:S(2)}, u32[]{:S(2)}) collective-permute-start(bf16[8,512]{1,0:T(8,128)(2,1)} %get-tuple-element.8), channel_id=1, source_target_pairs={{4,0},{8,4},{12,8},{5,1},{9,5},{13,9},{6,2},{10,6},{14,10},{7,3},{... | collective-permute-start | bytes 24584 | tf_op jit(solution)/shard_map/ppermute | solution.py:19
  235.4 8.7 %collective-permute-start.2 = (bf16[8,512]{1,0:T(8,128)(2,1)}, bf16[8,512]{1,0:T(8,128)(2,1)S(1)}, u32[]{:S(2)}, u32[]{:S(2)}) collective-permute-start(bf16[8,512]{1,0:T(8,128)(2,1)} %get-tuple-element.7), channel_id=1, source_target_pairs={{0,4},{4,8},{8,12},{1,5},{5,9},{9,13},{2,6},{6,10},{10,14},{3,7},{... | collective-permute-start | bytes 24584 | tf_op jit(solution)/shard_map/ppermute | solution.py:18
Sparse Core Ops, SparseCore 0:
  8.9 83.4 all-gather.3
  94.0 79.2 all-gather.5
  187.4 41.3 all-reduce.2
  257.1 41.9 all-reduce.4
